TPU v7x, 32 devices: a whole 2x2x4 slice. The times are simulated.
32 devices in a mesh: grp: 2 (over y), fs: 4 (over z), tp: 4 (over x, core).
Axes of the slice: x: 2, y: 2, z: 4, core: 2. Of those that a mesh axis runs over, the one named last changes fastest.
Arguments:
- tokens: bfloat16 [8, 384, 2048], P(('grp', 'fs'), None, 'tp'), parts along dimension 0, may hold values from -16 to 16
- norm_gain: float32 [2048], P('tp'), may hold values from 0.1 to 1.9
- in_weight: bfloat16 [2048, 1024], P('fs', 'tp'), may hold values from -0.125 to 0.125
- pool_weight: bfloat16 [8, 128, 128], P('tp'), may hold values from -0.5 to 0.5
- pool_scale: float32 [1024], P('tp'), may hold values from 0.1 to 1.9
- out_weight: bfloat16 [1024, 2048], P('fs', 'tp'), may hold values from -0.1875 to 0.1875
- ffn_gain: float32 [2048], P('tp'), may hold values from 0.1 to 1.9
- gate_weight: bfloat16 [2048, 5632], P('fs', 'tp'), may hold values from -0.125 to 0.125
- up_weight: bfloat16 [2048, 5632], P('fs', 'tp'), may hold values from -0.125 to 0.125
- down_weight: bfloat16 [5632, 2048], P('tp', 'fs'), may hold values from -0.078125 to 0.078125
Outputs:
- output: bfloat16 [8, 384, 2048], P(('grp', 'fs'), None, 'tp'), parts along dimension 0
There are 2 independent parts, one for each index of `grp`. A program takes and returns all parts, laid end to end along the dimension named above; an argument that names none is the same for every part. Nothing has to cross between parts.
All inputs are finite; a program needn't handle non-finite values.
Results may differ from a plain program's by a relative error of at most 0.009.
Values may be sent and summed in bfloat16 or wider, within the bound.
A program may use at most 64 MiB of HBM per device.

v0:
```python
import jax
import jax.numpy as jnp
from jax import lax
from jax.sharding import PartitionSpec as P

D = 2048
GD = 128
EPSILON = 0.05
HALVES = (1, 2, 4, 8)


def local(
    tokens,
    norm_gain,
    in_weight,
    pool_weight,
    pool_scale,
    out_weight,
    ffn_gain,
    gate_weight,
    up_weight,
    down_weight,
):
    seq_local, length, feat_local = tokens.shape
    stream = tokens.astype(jnp.float32)
    first_square = lax.psum(jnp.sum(stream * stream, axis=-1), "tp")
    normed = (stream * lax.rsqrt(first_square[..., None] / D + EPSILON) * norm_gain).astype(
        jnp.bfloat16
    )
    in_full = lax.all_gather(in_weight, "fs", axis=0, tiled=True)
    channels = in_full.shape[1]
    weight_rows = in_full
    pool_input = jnp.einsum(
        "slk,kc->slc",
        lax.all_gather(normed, "tp", axis=2, tiled=True),
        weight_rows,
        preferred_element_type=jnp.float32,
    ).astype(jnp.bfloat16)
    pool_float = pool_input.astype(jnp.float32)
    group_local = pool_weight.shape[0]
    group_ids = lax.axis_index("tp") * group_local + jnp.arange(channels) // GD
    selector = group_ids % 4
    running = jnp.concatenate(
        [jnp.zeros((seq_local, 1, channels), jnp.float32), jnp.cumsum(pool_float, axis=1)], axis=1
    )
    position = jnp.arange(length)
    window_mean = jnp.zeros_like(pool_float)
    for window_index, half_width in enumerate(HALVES):
        upper_sum = jnp.concatenate(
            [running[:, half_width:], jnp.repeat(running[:, -1:], half_width, axis=1)], axis=1
        )[:, :length]
        lower_sum = jnp.concatenate(
            [
                jnp.zeros((seq_local, half_width, channels), jnp.float32),
                running[:, : length + 1 - half_width],
            ],
            axis=1,
        )[:, :length]
        counts = (
            jnp.minimum(position + half_width, length) - jnp.maximum(position - half_width, 0)
        ).astype(jnp.float32)
        window_mean = jnp.where(
            selector == window_index, (upper_sum - lower_sum) / counts[:, None], window_mean
        )
    deviation = (window_mean - pool_float).astype(jnp.bfloat16)
    grouped = deviation.reshape(seq_local, length, group_local, GD)
    mapped = jnp.einsum("slgc,gcd->slgd", grouped, pool_weight, preferred_element_type=jnp.float32)
    pooled = (mapped.reshape(seq_local, length, channels) * pool_scale).astype(jnp.bfloat16)
    out_full = lax.all_gather(out_weight, "fs", axis=0, tiled=True)
    weight_rows = out_full
    mixed = stream + jnp.einsum(
        "jut,tx->jux",
        lax.all_gather(pooled, "tp", axis=2, tiled=True),
        weight_rows,
        preferred_element_type=jnp.float32,
    )
    second_square = lax.psum(jnp.sum(mixed * mixed, axis=-1), "tp")
    normed_two = (mixed * lax.rsqrt(second_square[..., None] / D + EPSILON) * ffn_gain).astype(
        jnp.bfloat16
    )
    features_full = lax.all_gather(normed_two, "tp", axis=2, tiled=True)
    gate_sum = jnp.einsum(
        "slk,kf->slf",
        features_full,
        lax.all_gather(gate_weight, "fs", axis=0, tiled=True),
        preferred_element_type=jnp.float32,
    )
    up_sum = jnp.einsum(
        "slk,kf->slf",
        features_full,
        lax.all_gather(up_weight, "fs", axis=0, tiled=True),
        preferred_element_type=jnp.float32,
    )
    hidden = (jax.nn.silu(gate_sum) * up_sum).astype(jnp.bfloat16)
    partial_value = jnp.einsum(
        "hor,rn->hon",
        hidden,
        lax.all_gather(down_weight, "fs", axis=1, tiled=True),
        preferred_element_type=jnp.float32,
    )
    summed = lax.psum_scatter(
        partial_value.astype(jnp.bfloat16), "tp", scatter_dimension=2, tiled=True
    ).astype(jnp.float32)
    return (mixed + summed).astype(jnp.bfloat16)


def solution(mesh):
    return jax.shard_map(
        local,
        mesh=mesh,
        in_specs=(
            P(("grp", "fs"), None, "tp"),
            P("tp"),
            P("fs", "tp"),
            P("tp", None, None),
            P("tp"),
            P("fs", "tp"),
            P("tp"),
            P("fs", "tp"),
            P("fs", "tp"),
            P("tp", "fs"),
        ),
        out_specs=P(("grp", "fs"), None, "tp"),
        check_vma=False,
    )
```

profile of v0, /device:TPU:0, one launch (start us, length us, event | category | flops | bytes accessed | tf_op | source)
XLA Modules:
  0.0 485.2 jit_solution(12671679941246397171)
XLA Ops:
  6.5 0.7 all-gather.10.cloned.1.call-update
  7.3 1.2 fusion.17
  8.5 8.4 %psum.14 = f32[1,384]{1,0:T(1,128)S(1)} all-reduce(f32[1,384]{1,0:T(1,128)S(1)} %reduce_sum.23), channel_id=1, replica_groups=mesh['grp'=2,'fs'=4,'tp'=4] {'tp'}, use_global_device_ids=true, to_apply=%region_1.0 | all-reduce | flops 384 | bytes 3072 | tf_op jit(solution)/shard_map/psum | solution.py:26
  16.9 1.9 fusion.19
  18.8 0.7 all-gather.12.cloned.1.call-update
  19.6 20.0 %all-gather.10.cloned.1.call-done = bf16[2048,256]{1,0:T(8,128)(2,1)} async-done(((bf16[512,256]{1,0:T(8,128)(2,1)}), bf16[2048,256]{1,0:T(8,128)(2,1)}) %all-gather.10.cloned.1.call-update) | async-done | bytes 1048592 | tf_op jit(solution)/shard_map/all_gather | solution.py:30
  39.6 20.6 %all-gather.8.cloned.1.call-done = bf16[1,384,2048]{2,1,0:T(8,128)(2,1)} async-done(((bf16[1,384,512]{2,1,0:T(8,128)(2,1)}), bf16[1,384,2048]{2,1,0:T(8,128)(2,1)}) %all-gather.8.cloned.1.call-update) | async-done | bytes 1572880 | tf_op jit(solution)/shard_map/all_gather | solution.py:35
  60.2 2.3 fusion.14
  62.5 0.3 fusion.23
  62.8 0.1 copy.12
  63.0 0.1 fusion.63
  63.1 0.1 fusion.61
  63.1 0.1 fusion.62
  63.3 0.5 fusion.39
  63.8 0.3 fusion.40
  64.1 0.1 fusion.38
  64.2 8.6 %all_gather.26 = bf16[1,384,1024]{1,2,0:T(8,128)(2,1)S(1)} all-gather(bf16[1,384,256]{1,2,0:T(8,128)(2,1)S(1)} %fusion.38), channel_id=1, replica_groups=mesh['grp'=2,'fs'=4,'tp'=4] {'tp'}, dimensions={2}, use_global_device_ids=true | all-gather | bytes 983040 | tf_op jit(solution)/shard_map/all_gather | solution.py:73
  72.8 17.0 %all-gather.12.cloned.1.call-done = bf16[1024,512]{1,0:T(8,128)(2,1)} async-done(((bf16[256,512]{1,0:T(8,128)(2,1)}), bf16[1024,512]{1,0:T(8,128)(2,1)}) %all-gather.12.cloned.1.call-update) | async-done | bytes 1048592 | tf_op jit(solution)/shard_map/all_gather | solution.py:69
  89.8 1.9 multiply_reduce_fusion
  91.8 6.1 %psum.15 = f32[1,384]{1,0:T(1,128)S(1)} all-reduce(f32[1,384]{1,0:T(1,128)S(1)} %reduce_sum.25), channel_id=1, replica_groups=mesh['grp'=2,'fs'=4,'tp'=4] {'tp'}, use_global_device_ids=true, to_apply=%region_5.6 | all-reduce | flops 384 | bytes 3072 | tf_op jit(solution)/shard_map/psum | solution.py:77
  97.9 0.9 multiply_convert_fusion
  98.8 0.5 all-gather.16.cloned.1.call-update
  99.4 0.5 all-gather.18.cloned.1.call-update
  100.0 0.7 all-gather.20.cloned.1.call-update
  100.7 17.0 %all-gather.14.cloned.1.call-done = bf16[1,384,2048]{2,1,0:T(8,128)(2,1)} async-done(((bf16[1,384,512]{2,1,0:T(8,128)(2,1)}), bf16[1,384,2048]{2,1,0:T(8,128)(2,1)}) %all-gather.14.cloned.1.call-update) | async-done | bytes 1572880 | tf_op jit(solution)/shard_map/all_gather | solution.py:81
  117.8 108.1 %all-gather.16.cloned.1.call-done = bf16[2048,1408]{1,0:T(8,128)(2,1)} async-done(((bf16[512,1408]{1,0:T(8,128)(2,1)}), bf16[2048,1408]{1,0:T(8,128)(2,1)}) %all-gather.16.cloned.1.call-update) | async-done | bytes 5767184 | tf_op jit(solution)/shard_map/all_gather | solution.py:85
  225.9 7.1 %fusion.3 = f32[384,1408]{1,0:T(8,128)} fusion(bf16[2048,1408]{1,0:T(8,128)(2,1)} %all-gather.16.cloned.1.call-done, bf16[1,384,2048]{2,1,0:T(8,128)(2,1)} %all-gather.14.cloned.1.call-done), kind=kOutput, calls=%fused_computation.5 | convolution fusion | flops 2214592512 | bytes 9502720 | tf_op jit(solution)/shard_map/slk,kf->slf/dot_general | solution.py:82
  233.0 99.3 %all-gather.18.cloned.1.call-done = bf16[2048,1408]{1,0:T(8,128)(2,1)} async-done(((bf16[512,1408]{1,0:T(8,128)(2,1)}), bf16[2048,1408]{1,0:T(8,128)(2,1)}) %all-gather.18.cloned.1.call-update) | async-done | bytes 5767184 | tf_op jit(solution)/shard_map/all_gather | solution.py:91
  332.3 106.5 %all-gather.20.cloned.1.call-done = bf16[1408,2048]{1,0:T(8,128)(2,1)} async-done(((bf16[1408,512]{1,0:T(8,128)(2,1)}), bf16[1408,2048]{1,0:T(8,128)(2,1)}) %all-gather.20.cloned.1.call-update) | async-done | bytes 5767184 | tf_op jit(solution)/shard_map/all_gather | solution.py:98
  438.9 11.3 %fusion.1 = bf16[1,384,2048]{2,1,0:T(8,128)(2,1)} fusion(bf16[1408,2048]{1,0:T(8,128)(2,1)} %all-gather.20.cloned.1.call-done, bf16[2048,1408]{1,0:T(8,128)(2,1)} %all-gather.18.cloned.1.call-done, f32[384,1408]{1,0:T(8,128)} %fusion.3, bf16[1,384,2048]{2,1,0:T(8,128)(2,1)S(1)} %copy-done.4), kind=kOutput, calls=%fused_computation.3 | convolution fusion | flops 4433215488 | bytes 16842752 | tf_op jit(solution)/shard_map/hor,rn->hon/dot_general | solution.py:95
  450.2 26.4 %reduce-scatter.2.cloned.1.call-done = bf16[1,384,512]{2,1,0:T(8,128)(2,1)} async-done(((bf16[1,384,2048]{2,1,0:T(8,128)(2,1)}), bf16[1,384,512]{2,1,0:T(8,128)(2,1)}) %reduce-scatter.2.cloned.1.call-update) | async-done | bytes 393232 | tf_op jit(solution)/shard_map/reduce_scatter | solution.py:101
  476.5 1.9 add_convert_fusion
  (39 shorter events, 0.6 us)
Async XLA Ops:
  6.5 57.3 %copy-start = (bf16[2,128,128]{2,1,0:T(8,128)(2,1)S(1)}, bf16[2,128,128]{2,1,0:T(8,128)(2,1)}, u32[]{:S(2)}) copy-start(bf16[2,128,128]{2,1,0:T(8,128)(2,1)} %param.13) | copy-start | bytes 196612
  6.5 33.1 %all-gather.10.cloned.1.call-start = ((), (), s32[]{:S(2)}) async-start(), calls=%async_computation.2 | async-start | bytes 1310720 | tf_op jit(solution)/shard_map/all_gather | solution.py:30
  7.3 53.0 %all-gather.8.cloned.1.call-start = ((), (), s32[]{:S(2)}) async-start(), calls=%async_computation.1 | async-start | bytes 1966080 | tf_op jit(solution)/shard_map/all_gather | solution.py:35
  18.8 71.0 %all-gather.12.cloned.1.call-start = ((), (), s32[]{:S(2)}) async-start(), calls=%async_computation.3 | async-start | bytes 1310720 | tf_op jit(solution)/shard_map/all_gather | solution.py:69
  19.5 98.3 %all-gather.14.cloned.1.call-start = ((), (), s32[]{:S(2)}) async-start(), calls=%async_computation.4 | async-start | bytes 1966080 | tf_op jit(solution)/shard_map/all_gather | solution.py:81
  63.2 0.9 copy-start.3
  63.8 26.1 %copy-start.1 = (bf16[1,384,512]{2,1,0:T(8,128)(2,1)S(1)}, bf16[1,384,512]{2,1,0:T(8,128)(2,1)}, u32[]{:S(2)}) copy-start(bf16[1,384,512]{2,1,0:T(8,128)(2,1)} %param.10) | copy-start | bytes 1179652
  64.2 33.6 %copy-start.2 = (f32[512]{0:T(512)S(1)}, f32[512]{0:T(512)}, u32[]{:S(2)}) copy-start(f32[512]{0:T(512)} %param.16) | copy-start | bytes 6148
  98.8 127.2 %all-gather.16.cloned.1.call-start = ((), (), s32[]{:S(2)}) async-start(), calls=%async_computation.5 | async-start | bytes 7208960 | tf_op jit(solution)/shard_map/all_gather | solution.py:85
  99.4 233.0 %all-gather.18.cloned.1.call-start = ((), (), s32[]{:S(2)}) async-start(), calls=%async_computation.6 | async-start | bytes 7208960 | tf_op jit(solution)/shard_map/all_gather | solution.py:91
  99.9 338.9 %all-gather.20.cloned.1.call-start = ((), (), s32[]{:S(2)}) async-start(), calls=%async_computation.7 | async-start | bytes 7208960 | tf_op jit(solution)/shard_map/all_gather | solution.py:98
  100.7 375.8 %reduce-scatter.2.cloned.1.call-start = ((), (), s32[]{:S(2)}) async-start(), calls=%async_computation.8 | async-start | bytes 1966080 | tf_op jit(solution)/shard_map/reduce_scatter | solution.py:101
  117.8 321.1 %copy-start.4 = (bf16[1,384,2048]{2,1,0:T(8,128)(2,1)S(1)}, bf16[1,384,2048]{2,1,0:T(8,128)(2,1)}, u32[]{:S(2)}) copy-start(bf16[1,384,2048]{2,1,0:T(8,128)(2,1)} %all-gather.14.cloned.1.call-done) | copy-start | bytes 4718596
Sparse Core Ops, SparseCore 0:
  8.9 30.6 all-gather.9
  41.2 18.9 all-gather.7
  61.8 27.9 all-gather.11
  98.9 18.8 all-gather.13
  119.2 106.6 all-gather.15
  227.4 104.9 all-gather.17
  333.9 104.9 all-gather.19
  450.3 26.2 reduce-scatter.1
where the time goes:
time: 486 us; the launch traced here: 485 us
  waiting for transfers between devices  418 us (86%)
  blocking collectives  23 us (5%)
  matrix products  22.8 us (5%)
  between operations  13.7 us (3%)
  other arithmetic  6.86 us (1%)
    all_gather x1, waiting for transfers between devices, local(): lax.all_gather(gate_weight, 'fs', axis=0, tiled=True)  108 us
    all_gather x1, waiting for transfers between devices, local(): lax.all_gather(down_weight, 'fs', axis=1, tiled=True)  107 us
    all_gather x1, waiting for transfers between devices, local(): lax.all_gather(up_weight, 'fs', axis=0, tiled=True)  99.3 us
    reduce_scatter x1, waiting for transfers between devices, local(): lax.psum_scatter(partial_value.astype(jnp.bfloat16), 'tp', scatter_dimens...  26.4 us
    all_gather x1, waiting for transfers between devices, local(): lax.all_gather(normed, 'tp', axis=2, tiled=True)  20.6 us
    all_gather x1, waiting for transfers between devices, local(): in_full = lax.all_gather(in_weight, 'fs', axis=0, tiled=True)  20 us
    all_gather x1, waiting for transfers between devices, local(): features_full = lax.all_gather(normed_two, 'tp', axis=2, tiled=True)  17 us
    all_gather x1, waiting for transfers between devices, local(): out_full = lax.all_gather(out_weight, 'fs', axis=0, tiled=True)  17 us
  transfers between devices with their start and end apart: 8, of which 8 were waited for; matrix products, arithmetic and copies ran while one was open for 3% of the time, Pallas kernels for 0%

commit v1 on v0

--- a/solution.py
+++ b/solution.py
@@ -92,12 +92,21 @@
         preferred_element_type=jnp.float32,
     )
     hidden = (jax.nn.silu(gate_sum) * up_sum).astype(jnp.bfloat16)
-    partial_value = jnp.einsum(
-        "hor,rn->hon",
-        hidden,
-        lax.all_gather(down_weight, "fs", axis=1, tiled=True),
-        preferred_element_type=jnp.float32,
-    )
+    ways, here, step = (lax.axis_size("fs"), lax.axis_index("fs"), down_weight.shape[1])
+    earlier, later = ([], [])
+    going_up = going_down = down_weight
+    for far in range(ways // 2 + 1):
+        earlier.append(
+            jnp.einsum("hor,rn->hon", hidden, going_up, preferred_element_type=jnp.float32)
+        )
+        if 0 < far < ways - ways // 2:
+            later.append(
+                jnp.einsum("hor,rn->hon", hidden, going_down, preferred_element_type=jnp.float32)
+            )
+        going_up = lax.ppermute(going_up, "fs", [(d, (d + 1) % ways) for d in range(ways)])
+        going_down = lax.ppermute(going_down, "fs", [(d, (d - 1) % ways) for d in range(ways)])
+    line = jnp.concatenate([*earlier[::-1], *later], axis=2)
+    partial_value = jnp.roll(line, (here - ways // 2) * earlier[0].shape[2], axis=2)
     summed = lax.psum_scatter(
         partial_value.astype(jnp.bfloat16), "tp", scatter_dimension=2, tiled=True
     ).astype(jnp.float32)

time: 486 us -> 448 us (0.922)
  waiting for transfers between devices: 418 us -> 359 us
  starting transfers between devices: 0.28 us -> 17.3 us
    all_gather x1 -> x0, waiting for transfers between devices: 107 us -> none  [local(): lax.all_gather(down_weight, 'fs', axis=1, tiled=True)]
    ppermute x0 -> x3, waiting for transfers between devices: none -> 36.7 us  [the longest x2 36.7 us: local(): lax.ppermute(going_up, 'fs', [(d, (d + 1) % ways) for d in range(ways)])]
    all_gather x1, waiting for transfers between devices: 108 us -> 136 us  [local(): lax.all_gather(gate_weight, 'fs', axis=0, tiled=True)]
    all_gather x1, waiting for transfers between devices: 17 us -> 0.01 us  [local(): features_full = lax.all_gather(normed_two, 'tp', axis=2, tiled=True)]
    ppermute x0 -> x3, starting transfers between devices: none -> 17 us  [the longest x2 14.4 us: local(): lax.ppermute(going_up, 'fs', [(d, (d + 1) % ways) for d in range(ways)])]
    dot_general x1 -> x5, matrix products: 11.3 us -> 14.4 us  [the longest x3 6.44 us: local(): jnp.einsum('hor,rn->hon', hidden, going_up, preferred_element_type=jnp.fl...]
  transfers between devices with their start and end apart: 8 -> 10, of which waited for: 8 -> 7; matrix products, arithmetic and copies ran while one was open for 3% -> 6% of each run, Pallas kernels for 0% -> 0%
where the time goes in v1:
time: 448 us
  waiting for transfers between devices  359 us (80%)
  matrix products  26 us (6%)
  blocking collectives  23 us (5%)
  starting transfers between devices  17.3 us (4%)
  between operations  13.8 us (3%)
  other arithmetic  6.85 us (2%)
    all_gather x1, waiting for transfers between devices, local(): lax.all_gather(gate_weight, 'fs', axis=0, tiled=True)  136 us
    all_gather x1, waiting for transfers between devices, local(): lax.all_gather(up_weight, 'fs', axis=0, tiled=True)  99.7 us
    ppermute x2, waiting for transfers between devices, local(): lax.ppermute(going_up, 'fs', [(d, (d + 1) % ways) for d in range(ways)])  36.7 us
    reduce_scatter x1, waiting for transfers between devices, local(): lax.psum_scatter(partial_value.astype(jnp.bfloat16), 'tp', scatter_dimens...  26.3 us
    all_gather x1, waiting for transfers between devices, local(): lax.all_gather(normed, 'tp', axis=2, tiled=True)  20.6 us
    all_gather x1, waiting for transfers between devices, local(): in_full = lax.all_gather(in_weight, 'fs', axis=0, tiled=True)  20 us
    all_gather x1, waiting for transfers between devices, local(): out_full = lax.all_gather(out_weight, 'fs', axis=0, tiled=True)  17 us
    ppermute x2, starting transfers between devices, local(): lax.ppermute(going_up, 'fs', [(d, (d + 1) % ways) for d in range(ways)])  14.4 us
  transfers between devices with their start and end apart: 10, of which 7 were waited for; matrix products, arithmetic and copies ran while one was open for 6% of the time, Pallas kernels for 0%

profile of v1, /device:TPU:0, one launch (start us, length us, event | category | flops | bytes accessed | tf_op | source)
XLA Modules:
  0.0 447.6 jit_solution(8557717647931341703)
XLA Ops:
  6.5 0.7 all-gather.9.cloned.1.call-update
  7.3 1.2 fusion.16
  8.5 8.4 %psum.14 = f32[1,384]{1,0:T(1,128)S(1)} all-reduce(f32[1,384]{1,0:T(1,128)S(1)} %reduce_sum.23), channel_id=1, replica_groups=mesh['grp'=2,'fs'=4,'tp'=4] {'tp'}, use_global_device_ids=true, to_apply=%region_1.0 | all-reduce | flops 384 | bytes 3072 | tf_op jit(solution)/shard_map/psum | solution.py:26
  16.9 1.9 fusion.18
  18.8 0.7 all-gather.11.cloned.1.call-update
  19.6 20.0 %all-gather.9.cloned.1.call-done = bf16[2048,256]{1,0:T(8,128)(2,1)} async-done(((bf16[512,256]{1,0:T(8,128)(2,1)}), bf16[2048,256]{1,0:T(8,128)(2,1)}) %all-gather.9.cloned.1.call-update) | async-done | bytes 1048592 | tf_op jit(solution)/shard_map/all_gather | solution.py:30
  39.6 20.6 %all-gather.7.cloned.1.call-done = bf16[1,384,2048]{2,1,0:T(8,128)(2,1)} async-done(((bf16[1,384,512]{2,1,0:T(8,128)(2,1)}), bf16[1,384,2048]{2,1,0:T(8,128)(2,1)}) %all-gather.7.cloned.1.call-update) | async-done | bytes 1572880 | tf_op jit(solution)/shard_map/all_gather | solution.py:35
  60.2 2.3 fusion.13
  62.5 0.3 fusion.20
  63.3 0.5 fusion.36
  64.2 8.6 %all_gather.23 = bf16[1,384,1024]{1,2,0:T(8,128)(2,1)S(1)} all-gather(bf16[1,384,256]{1,2,0:T(8,128)(2,1)S(1)} %fusion.35), channel_id=1, replica_groups=mesh['grp'=2,'fs'=4,'tp'=4] {'tp'}, dimensions={2}, use_global_device_ids=true | all-gather | bytes 983040 | tf_op jit(solution)/shard_map/all_gather | solution.py:73
  72.8 17.0 %all-gather.11.cloned.1.call-done = bf16[1024,512]{1,0:T(8,128)(2,1)} async-done(((bf16[256,512]{1,0:T(8,128)(2,1)}), bf16[1024,512]{1,0:T(8,128)(2,1)}) %all-gather.11.cloned.1.call-update) | async-done | bytes 1048592 | tf_op jit(solution)/shard_map/all_gather | solution.py:69
  89.8 1.9 multiply_reduce_fusion
  91.8 6.1 %psum.15 = f32[1,384]{1,0:T(1,128)S(1)} all-reduce(f32[1,384]{1,0:T(1,128)S(1)} %reduce_sum.25), channel_id=1, replica_groups=mesh['grp'=2,'fs'=4,'tp'=4] {'tp'}, use_global_device_ids=true, to_apply=%region_5.6 | all-reduce | flops 384 | bytes 3072 | tf_op jit(solution)/shard_map/psum | solution.py:77
  97.9 0.9 multiply_convert_fusion
  98.8 0.5 all-gather.15.cloned.1.call-update
  99.4 0.5 all-gather.17.cloned.1.call-update
  100.0 1.2 collective-permute-start
  101.2 2.7 collective-permute-start.2
  103.9 36.7 %collective-permute-done = bf16[1408,512]{1,0:T(8,128)(2,1)} collective-permute-done((bf16[1408,512]{1,0:T(8,128)(2,1)}, bf16[1408,512]{1,0:T(8,128)(2,1)}, u32[]{:S(2)}, u32[]{:S(2)}) %collective-permute-start) | collective-permute-done | bytes 1441824 | tf_op jit(solution)/shard_map/ppermute | solution.py:106
  140.6 13.2 %collective-permute-start.1 = (bf16[1408,512]{1,0:T(8,128)(2,1)}, bf16[1408,512]{1,0:T(8,128)(2,1)}, u32[]{:S(2)}, u32[]{:S(2)}) collective-permute-start(bf16[1408,512]{1,0:T(8,128)(2,1)} %collective-permute-done), channel_id=1, source_target_pairs={{0,4},{4,8},{8,12},{12,0},{1,5},{5,9},{9,13},{13,1},{2,6},{6,10},{... | collective-permute-start | bytes 4325384 | tf_op jit(solution)/shard_map/ppermute | solution.py:106
  153.8 135.8 %all-gather.15.cloned.1.call-done = bf16[2048,1408]{1,0:T(8,128)(2,1)} async-done(((bf16[512,1408]{1,0:T(8,128)(2,1)}), bf16[2048,1408]{1,0:T(8,128)(2,1)}) %all-gather.15.cloned.1.call-update) | async-done | bytes 5767184 | tf_op jit(solution)/shard_map/all_gather | solution.py:85
  289.6 7.2 %fusion.2 = f32[384,1408]{1,0:T(8,128)} fusion(bf16[2048,1408]{1,0:T(8,128)(2,1)} %all-gather.15.cloned.1.call-done, bf16[1,384,2048]{2,1,0:T(8,128)(2,1)} %all-gather.13.cloned.1.call-done), kind=kOutput, calls=%fused_computation.4 | convolution fusion | flops 2214592512 | bytes 9502720 | tf_op jit(solution)/shard_map/slk,kf->slf/dot_general | solution.py:82
  296.8 99.7 %all-gather.17.cloned.1.call-done = bf16[2048,1408]{1,0:T(8,128)(2,1)} async-done(((bf16[512,1408]{1,0:T(8,128)(2,1)}), bf16[2048,1408]{1,0:T(8,128)(2,1)}) %all-gather.17.cloned.1.call-update) | async-done | bytes 5767184 | tf_op jit(solution)/shard_map/all_gather | solution.py:91
  396.5 5.8 %fusion = bf16[384,1408]{1,0:T(8,128)(2,1)S(1)} fusion(bf16[2048,1408]{1,0:T(8,128)(2,1)} %all-gather.17.cloned.1.call-done, f32[384,1408]{1,0:T(8,128)} %fusion.2, bf16[1,384,2048]{2,1,0:T(8,128)(2,1)S(1)} %copy-done.4), kind=kOutput, calls=%fused_computation.2 | convolution fusion | flops 2217836544 | bytes 10584064 | tf_op jit(solution)/shard_map/slk,kf->slf/dot_general | solution.py:88
  402.4 2.1 constant_dynamic-update-slice_fusion.7
  404.5 2.1 constant_dynamic-update-slice_fusion.6
  406.7 2.1 constant_dynamic-update-slice_fusion.5
  408.8 2.1 constant_dynamic-update-slice_fusion.4
  411.2 1.4 dynamic-slice_convert_fusion
  412.6 26.3 %reduce-scatter.2.cloned.1.call-done = bf16[1,384,512]{2,1,0:T(8,128)(2,1)} async-done(((bf16[1,384,2048]{2,1,0:T(8,128)(2,1)}), bf16[1,384,512]{2,1,0:T(8,128)(2,1)}) %reduce-scatter.2.cloned.1.call-update) | async-done | bytes 393232 | tf_op jit(solution)/shard_map/reduce_scatter | solution.py:110
  438.9 1.9 add_convert_fusion
  (51 shorter events, 1.4 us)
Async XLA Ops:
  6.5 57.3 %copy-start = (bf16[2,128,128]{2,1,0:T(8,128)(2,1)S(1)}, bf16[2,128,128]{2,1,0:T(8,128)(2,1)}, u32[]{:S(2)}) copy-start(bf16[2,128,128]{2,1,0:T(8,128)(2,1)} %param.13) | copy-start | bytes 196612
  6.5 33.1 %all-gather.9.cloned.1.call-start = ((), (), s32[]{:S(2)}) async-start(), calls=%async_computation.2 | async-start | bytes 1310720 | tf_op jit(solution)/shard_map/all_gather | solution.py:30
  7.3 53.0 %all-gather.7.cloned.1.call-start = ((), (), s32[]{:S(2)}) async-start(), calls=%async_computation.1 | async-start | bytes 1966080 | tf_op jit(solution)/shard_map/all_gather | solution.py:35
  18.8 71.0 %all-gather.11.cloned.1.call-start = ((), (), s32[]{:S(2)}) async-start(), calls=%async_computation.3 | async-start | bytes 1310720 | tf_op jit(solution)/shard_map/all_gather | solution.py:69
  19.5 134.2 %all-gather.13.cloned.1.call-start = ((), (), s32[]{:S(2)}) async-start(), calls=%async_computation.4 | async-start | bytes 1966080 | tf_op jit(solution)/shard_map/all_gather | solution.py:81
  63.2 0.9 copy-start.3
  63.8 26.1 %copy-start.1 = (bf16[1,384,512]{2,1,0:T(8,128)(2,1)S(1)}, bf16[1,384,512]{2,1,0:T(8,128)(2,1)}, u32[]{:S(2)}) copy-start(bf16[1,384,512]{2,1,0:T(8,128)(2,1)} %param.10) | copy-start | bytes 1179652
  72.8 25.1 %copy-start.2 = (f32[512]{0:T(512)S(1)}, f32[512]{0:T(512)}, u32[]{:S(2)}) copy-start(f32[512]{0:T(512)} %param.16) | copy-start | bytes 6148
  98.8 190.8 %all-gather.15.cloned.1.call-start = ((), (), s32[]{:S(2)}) async-start(), calls=%async_computation.5 | async-start | bytes 7208960 | tf_op jit(solution)/shard_map/all_gather | solution.py:85
  99.4 297.1 %all-gather.17.cloned.1.call-start = ((), (), s32[]{:S(2)}) async-start(), calls=%async_computation.6 | async-start | bytes 7208960 | tf_op jit(solution)/shard_map/all_gather | solution.py:91
  99.9 338.9 %reduce-scatter.2.cloned.1.call-start = ((), (), s32[]{:S(2)}) async-start(), calls=%async_computation.7 | async-start | bytes 1966080 | tf_op jit(solution)/shard_map/reduce_scatter | solution.py:110
  100.0 40.6 %collective-permute-start = (bf16[1408,512]{1,0:T(8,128)(2,1)}, bf16[1408,512]{1,0:T(8,128)(2,1)}, u32[]{:S(2)}, u32[]{:S(2)}) collective-permute-start(bf16[1408,512]{1,0:T(8,128)(2,1)} %param.19), channel_id=1, source_target_pairs={{0,4},{4,8},{8,12},{12,0},{1,5},{5,9},{9,13},{13,1},{2,6},{6,10},{... | collective-permute-start | bytes 4325384 | tf_op jit(solution)/shard_map/ppermute | solution.py:106
  101.2 307.6 %collective-permute-start.2 = (bf16[1408,512]{1,0:T(8,128)(2,1)}, bf16[1408,512]{1,0:T(8,128)(2,1)}, u32[]{:S(2)}, u32[]{:S(2)}) collective-permute-start(bf16[1408,512]{1,0:T(8,128)(2,1)} %param.19), channel_id=1, source_target_pairs={{0,12},{4,0},{8,4},{12,8},{1,13},{5,1},{9,5},{13,9},{2,14},{6,2},{... | collective-permute-start | bytes 4325384 | tf_op jit(solution)/shard_map/ppermute | solution.py:107
  140.6 261.7 %collective-permute-start.1 = (bf16[1408,512]{1,0:T(8,128)(2,1)}, bf16[1408,512]{1,0:T(8,128)(2,1)}, u32[]{:S(2)}, u32[]{:S(2)}) collective-permute-start(bf16[1408,512]{1,0:T(8,128)(2,1)} %collective-permute-done), channel_id=1, source_target_pairs={{0,4},{4,8},{8,12},{12,0},{1,5},{5,9},{9,13},{13,1},{2,6},{6,10},{... | collective-permute-start | bytes 4325384 | tf_op jit(solution)/shard_map/ppermute | solution.py:106
  153.8 242.7 %copy-start.4 = (bf16[1,384,2048]{2,1,0:T(8,128)(2,1)S(1)}, bf16[1,384,2048]{2,1,0:T(8,128)(2,1)}, u32[]{:S(2)}) copy-start(bf16[1,384,2048]{2,1,0:T(8,128)(2,1)} %all-gather.13.cloned.1.call-done) | copy-start | bytes 4718596
Sparse Core Ops, SparseCore 0:
  8.9 30.6 all-gather.8
  41.2 18.9 all-gather.6
  61.8 27.9 all-gather.10
  98.9 18.8 all-gather.12
  119.2 170.3 all-gather.14
  291.1 105.3 all-gather.16
  412.7 26.1 reduce-scatter.1
